TPU v7x, 32 devices: a whole 2x2x4 slice. The times are simulated.
32 devices in a mesh: sp: 4 (over z), fs: 4 (over y, x), tp: 2 (over core).
Axes of the slice: x: 2, y: 2, z: 4, core: 2. Of those that a mesh axis runs over, the one named last changes fastest.
Arguments:
- tokens: bfloat16 [4, 2048, 2048], P('fs', 'sp', 'tp'), may hold values from -6 to 6
- norm_gain: float32 [2048], replicated, may hold values from 0.1 to 1.9
- w_pool_in: bfloat16 [2048, 512], P('fs', 'tp'), may hold values from -0.125 to 0.125
- w_query: bfloat16 [2048, 1024], P('fs', 'tp'), may hold values from -0.125 to 0.125
- w_key: bfloat16 [2048, 1024], P('fs', 'tp'), may hold values from -0.125 to 0.125
- w_value: bfloat16 [2048, 1024], P('fs', 'tp'), may hold values from -0.125 to 0.125
- query_gain: float32 [64], replicated, may hold values from 1.5 to 2.5
- key_gain: float32 [64], replicated, may hold values from 1.5 to 2.5
- stick_offset: float32 [16], P('tp'), as said below
- pool_mix: bfloat16 [4, 128, 128], P('tp'), may hold values from -0.5 to 0.5
- pool_scale: float32 [512], P('tp'), may hold values from 0.2 to 4, as said below
- pool_gain: bfloat16 [512], P('tp'), may hold values from 0.099609375 to 1.8984375
- attn_gain: bfloat16 [1024], P('tp'), may hold values from 0.099609375 to 1.8984375
- w_out_pool: bfloat16 [512, 2048], P('tp', 'fs'), may hold values from -0.15625 to 0.15625
- w_out_attn: bfloat16 [1024, 2048], P('tp', 'fs'), may hold values from -0.15625 to 0.15625
Outputs:
- mixed: bfloat16 [4, 2048, 2048], P('fs', ('sp', 'tp'))
Inputs may be any that keep to these rules, and one draw needn't show every extreme that they name: `stick_offset`: per head, negative. `pool_scale`: positive channel scales.
All inputs are finite; a program needn't handle non-finite values.
Results may differ from a plain program's by a relative error of at most 0.013.
Values may be sent and summed in bfloat16 or wider, within the bound.
A program may use at most 192 MiB of HBM per device.

v0:
```python
import math

import jax
import jax.numpy as jnp
from jax import lax
from jax.sharding import PartitionSpec as P

HEADS = 16
HEAD_DIM = 64
POOL = 512
POOL_GROUPS = 4


EPS = 1e-06


def shifted_2(value, axis, steps):
    count = lax.axis_size(axis)
    initial, last = (max(0, -steps), min(count, count - steps))
    return lax.ppermute(value, axis, [(source, source + steps) for source in range(initial, last)])


def head_norm(projected, gain, head_count):
    split = projected.reshape(projected.shape[0], head_count, HEAD_DIM)
    factor = lax.rsqrt(jnp.mean(split * split, axis=-1, keepdims=True) + EPS)
    return (split * factor * gain).astype(jnp.bfloat16)


def stick_block(query, key_heads, value_heads, offset, carried, row_offset, score_scale):
    scores = (
        jnp.einsum("thd,khd->htk", query, key_heads, preferred_element_type=jnp.float32)
        * score_scale
        + offset[:, None, None]
    )
    keep = jax.nn.log_sigmoid(-scores)
    if row_offset is not None:
        shape = (query.shape[0], key_heads.shape[0])
        earlier = (
            lax.broadcasted_iota(jnp.int32, shape, 1)
            < lax.broadcasted_iota(jnp.int32, shape, 0) + row_offset
        )
        keep = jnp.where(earlier[None], keep, 0.0)
    running = jnp.cumsum(keep, axis=2)
    block_total = running[:, :, -1]
    log_weight = (
        jax.nn.log_sigmoid(scores) + block_total[:, :, None] - running + carried[:, :, None]
    )
    weight = jnp.exp(log_weight)
    if row_offset is not None:
        weight = jnp.where(earlier[None], weight, 0.0)
    weight = weight.astype(jnp.bfloat16)
    block_out = jnp.einsum("htk,khd->thd", weight, value_heads, preferred_element_type=jnp.float32)
    return (block_out, block_total)


def branch_norm(values_in, squares, width, gain):
    values_f = values_in.astype(jnp.float32)
    factor = lax.rsqrt(squares / width + EPS)
    return (values_f * factor[:, None] * gain.astype(jnp.float32)).astype(jnp.bfloat16)


def shards(
    tokens,
    norm_gain,
    w_pool_in,
    w_query,
    w_key,
    w_value,
    query_gain,
    key_gain,
    stick_offset,
    pool_mix,
    pool_scale,
    pool_gain,
    attn_gain,
    w_out_pool,
    w_out_attn,
):
    whole = lax.all_gather(tokens, "tp", axis=2, tiled=True)[0]
    whole_f = whole.astype(jnp.float32)
    normed = (
        whole_f * lax.rsqrt(jnp.mean(whole_f * whole_f, axis=-1, keepdims=True) + EPS) * norm_gain
    ).astype(jnp.bfloat16)
    row_count = normed.shape[0]
    pieces = (
        lax.all_gather(w_pool_in, "fs", axis=0, tiled=True),
        lax.all_gather(w_query, "fs", axis=0, tiled=True),
        lax.all_gather(w_key, "fs", axis=0, tiled=True),
        lax.all_gather(w_value, "fs", axis=0, tiled=True),
    )
    pool_raw, query_raw, key_raw, value_raw = tuple(
        (jnp.dot(normed, piece, preferred_element_type=jnp.float32) for piece in pieces)
    )
    head_count = query_raw.shape[1] // HEAD_DIM
    query = head_norm(query_raw, query_gain, head_count)
    key_heads = head_norm(key_raw, key_gain, head_count)
    value_heads = value_raw.astype(jnp.bfloat16).reshape(row_count, head_count, HEAD_DIM)
    reach = 16
    pool_in = pool_raw.astype(jnp.bfloat16)
    previous = shifted_2(pool_in[row_count - reach :], "sp", 1)
    extended = jnp.concatenate([previous, pool_in], axis=0).astype(jnp.float32)
    pool_cols = pool_in.shape[1]
    group_ch = POOL // POOL_GROUPS
    local_groups = pool_cols // group_ch
    group_ids = (
        lax.axis_index("tp") * local_groups + jnp.arange(pool_cols, dtype=jnp.int32) // group_ch
    )
    window = jnp.left_shift(jnp.int32(2), group_ids)
    summed = jnp.zeros((row_count, pool_cols), jnp.float32)
    for behind in range(reach):
        shifted = extended[reach - behind : reach - behind + row_count]
        summed = summed + jnp.where(behind < window[None, :], shifted, 0.0)
    sp_index = lax.axis_index("sp")
    position = sp_index * row_count + jnp.arange(row_count, dtype=jnp.int32)
    counted = jnp.minimum(position[:, None] + 1, window[None, :]).astype(jnp.float32)
    centered = (summed / counted - extended[reach:]).astype(jnp.bfloat16)
    pooled = jnp.einsum(
        "tgc,gcd->tgd",
        centered.reshape(row_count, local_groups, group_ch),
        pool_mix,
        preferred_element_type=jnp.float32,
    )
    pool_out = (pooled.reshape(row_count, pool_cols) * pool_scale).astype(jnp.bfloat16)
    score_scale = 1.0 / math.sqrt(HEAD_DIM)
    sp_count = lax.axis_size("sp")
    key_value = jnp.stack([key_heads, value_heads])
    start_carry = jnp.zeros((head_count, row_count), jnp.float32)
    output, carried = stick_block(
        query, key_heads, value_heads, stick_offset, start_carry, 0, score_scale
    )
    everything = lax.all_gather(key_value, "sp", axis=1, tiled=True)

    def turn(turn_index, state):
        acc_out, acc_carry = state
        source = jnp.maximum(sp_index - turn_index, 0)
        block = lax.dynamic_slice_in_dim(everything, source * row_count, row_count, 1)
        block_out, block_total = stick_block(
            query, block[0], block[1], stick_offset, acc_carry, None, score_scale
        )
        usable = turn_index <= sp_index
        return (
            acc_out + jnp.where(usable, block_out, 0.0),
            acc_carry + jnp.where(usable, block_total, 0.0),
        )

    output, carried = lax.fori_loop(1, sp_count, turn, (output, carried))
    attn_out = output.reshape(row_count, head_count * HEAD_DIM).astype(jnp.bfloat16)
    w_pool_cols, w_attn_cols = (
        lax.all_gather(w_out_pool, "fs", axis=1, tiled=True),
        lax.all_gather(w_out_attn, "fs", axis=1, tiled=True),
    )
    pool_f = pool_out.astype(jnp.float32)
    attn_f = attn_out.astype(jnp.float32)
    pool_sq, attn_sq = lax.psum(
        (jnp.sum(pool_f * pool_f, axis=-1), jnp.sum(attn_f * attn_f, axis=-1)), "tp"
    )
    pool_normed = branch_norm(pool_out, pool_sq, POOL, pool_gain)
    attn_normed = branch_norm(attn_out, attn_sq, HEADS * HEAD_DIM, attn_gain)
    mixed = lax.psum_scatter(
        (
            jnp.dot(pool_normed, w_pool_cols, preferred_element_type=jnp.float32)
            + jnp.dot(attn_normed, w_attn_cols, preferred_element_type=jnp.float32)
        ).astype(jnp.bfloat16),
        "tp",
        scatter_dimension=0,
        tiled=True,
    )
    return mixed[None]


def solution(mesh):
    in_specs = (
        P("fs", "sp", "tp"),
        P(),
        P("fs", "tp"),
        P("fs", "tp"),
        P("fs", "tp"),
        P("fs", "tp"),
        P(),
        P(),
        P("tp"),
        P("tp", None, None),
        P("tp"),
        P("tp"),
        P("tp"),
        P("tp", "fs"),
        P("tp", "fs"),
    )
    out_specs = P("fs", ("sp", "tp"), None)
    return jax.shard_map(shards, mesh=mesh, in_specs=in_specs, out_specs=out_specs, check_vma=False)
```

profile of v0, /device:TPU:0, one launch (start us, length us, event | category | flops | bytes accessed | tf_op | source)
XLA Modules:
  0.0 412.5 jit_solution(4075193351739934598)
XLA Ops:
  6.5 0.7 all-gather.9.cloned.1.call-update
  7.3 0.7 all-gather.19.cloned.1.call-update
  8.1 0.7 all-gather.15.cloned.1.call-update
  8.8 0.5 all-gather.11.cloned.1.call-update
  9.4 0.5 all-gather.17.cloned.1.call-update
  10.0 12.2 %all-gather.9.cloned.1.call-done = bf16[1,512,2048]{2,1,0:T(8,128)(2,1)} async-done(((bf16[1,512,1024]{2,1,0:T(8,128)(2,1)}), bf16[1,512,2048]{2,1,0:T(8,128)(2,1)}) %all-gather.9.cloned.1.call-update) | async-done | bytes 2097168 | tf_op jit(solution)/shard_map/all_gather | solution.py:79
  22.2 2.1 fusion.42
  24.3 36.1 %all-gather.19.cloned.1.call-done = bf16[2048,512]{1,0:T(8,128)(2,1)} async-done(((bf16[512,512]{1,0:T(8,128)(2,1)}), bf16[2048,512]{1,0:T(8,128)(2,1)}) %all-gather.19.cloned.1.call-update) | async-done | bytes 2097168 | tf_op jit(solution)/shard_map/all_gather | solution.py:88
  60.4 4.0 copy.22
  64.4 3.6 multiply_reduce_fusion.1
  68.0 0.9 copy-done.5
  69.0 0.2 fusion.93
  69.2 28.3 %all-gather.15.cloned.1.call-done = bf16[2048,512]{1,0:T(8,128)(2,1)} async-done(((bf16[512,512]{1,0:T(8,128)(2,1)}), bf16[2048,512]{1,0:T(8,128)(2,1)}) %all-gather.15.cloned.1.call-update) | async-done | bytes 2097168 | tf_op jit(solution)/shard_map/all_gather | solution.py:89
  97.5 3.0 convolution_convert_fusion
  100.5 0.8 copy-done.7
  101.3 1.1 pad_maximum_fusion
  102.5 0.7 all-gather.13.cloned.1.call-update
  103.2 0.7 all-gather.23.cloned.1.call-update
  104.2 21.5 %all-gather.11.cloned.1.call-done = bf16[2048,256]{1,0:T(8,128)(2,1)} async-done(((bf16[512,256]{1,0:T(8,128)(2,1)}), bf16[2048,256]{1,0:T(8,128)(2,1)}) %all-gather.11.cloned.1.call-update) | async-done | bytes 1048592 | tf_op jit(solution)/shard_map/all_gather | solution.py:86
  125.7 2.0 convolution_convert_fusion.1
  127.7 3.9 collective-permute-start
  131.6 0.5 convert_element_type.104
  132.1 0.6 convert_element_type.117
  132.8 2.1 multiply_reduce_fusion.3
  134.9 0.8 fusion.78
  135.7 26.9 %all-gather.17.cloned.1.call-done = bf16[2048,512]{1,0:T(8,128)(2,1)} async-done(((bf16[512,512]{1,0:T(8,128)(2,1)}), bf16[2048,512]{1,0:T(8,128)(2,1)}) %all-gather.17.cloned.1.call-update) | async-done | bytes 2097168 | tf_op jit(solution)/shard_map/all_gather | solution.py:87
  162.6 4.0 copy.21
  166.6 3.0 multiply_reduce_fusion.2
  169.6 0.2 multiply_convert_fusion.1
  169.8 10.2 %fusion.37 = (f32[8,512,512]{1,2,0:T(8,128)}, f32[8,512,512]{1,2,0:T(8,128)}) fusion(f32[8]{0:T(128)S(1)} %copy-done.18, pred[512,512]{0,1:T(8,128)(4,1)S(1)} %iota_compare_fusion, bf16[512,8,64]{0,2,1:T(8,128)(2,1)S(1)} %multiply_convert_fusion.1, f32[512,8,64]{0,2,1:T(8,128)S(1)} %copy-done.6, f32[64]{0:T(128)S(1)} %copy-done.15, ...), kind=kOutput, calls=%fused_computation.44 | convolution fusion | flops 290193408 | bytes 18628896 | tf_op jit(solution)/shard_map/thd,khd->htk/dot_general | solution.py:31
  180.0 11.5 %fusion.38 = f32[8,512,4,128]{1,0,3,2:T(8,128)} fusion(f32[8,512,4,128]{1,3,2,0:T(8,128)} %bitcast.155), kind=kOutput, calls=%fused_computation.45 | output fusion | flops 266338304 | bytes 16777216 | tf_op jit(solution)/shard_map/reduce-window
  191.6 0.8 fusion.88
  192.4 4.4 %broadcast_add_fusion.1 = f32[8,512,4,128]{1,0,3,2:T(8,128)S(1)} fusion(f32[8,512,4,128]{1,0,3,2:T(8,128)} %fusion.38, f32[8,512,4]{1,0,2:T(8,128)S(1)} %slice.133), kind=kLoop, calls=%fused_computation.58 | loop fusion | flops 2097152 | bytes 16842752 | tf_op jit(solution)/shard_map/reduce_window_sum
  196.9 4.9 %copy.24 = f32[8,512,4,128]{1,3,2,0:T(8,128)S(1)} copy(f32[8,512,4,128]{1,0,3,2:T(8,128)S(1)} %broadcast_add_fusion.1) | data formatting | bytes 16777216 | tf_op jit(solution)/shard_map/reduce_window_sum
  201.8 9.5 %fusion.50 = f32[512,8,64]{0,2,1:T(8,128)S(1)} fusion(bf16[512,8,64]{0,2,1:T(8,128)(2,1)S(1)} %bitcast.163, f32[8,512,512]{1,2,0:T(8,128)S(1)} %bitcast.154, f32[8,512,512]{1,2,0:T(8,128)} %get-tuple-element.157, f32[8,512]{1,0:T(8,128)S(1)} %bitcast.160, f32[8]{0:T(128)S(1)} %copy-done.18, pred[512,512]{0,1:T(8,128)(4,1)S(1)} %iota_compare_fusion), kind=kOutput, calls=%fused_computation.61 | convolution fusion | flops 297795584 | bytes 18628640 | tf_op jit(solution)/shard_map/htk,khd->thd/dot_general | solution.py:52
  211.3 33.6 %all-gather.21.cloned.1.call-done = bf16[2,2048,8,64]{1,3,2,0:T(8,128)(2,1)} async-done(((bf16[2,512,8,64]{1,3,2,0:T(8,128)(2,1)}), bf16[2,2048,8,64]{1,3,2,0:T(8,128)(2,1)}) %all-gather.21.cloned.1.call-update) | async-done | bytes 4194320 | tf_op jit(solution)/shard_map/all_gather | solution.py:131
  244.8 139.7 %while.15 = (s32[]{:T(128)}, f32[512,8,64]{0,2,1:T(8,128)S(1)}, f32[8,512]{1,0:T(8,128)S(1)}, s32[]{:T(128)}, bf16[2,2048,8,64]{1,3,2,0:T(8,128)(2,1)}, /*index=...) while((s32[]{:T(128)}, f32[512,8,64]{0,2,1:T(8,128)S(1)}, ...), condition=%wide.region_10.11_spmd, body=%wide.region_7.10_spmd.sunk | while | flops 854134784 | bytes 121602360 | solution.py:146
  245.1 10.4 %fusion.118 = (f32[8,512,512]{1,2,0:T(8,128)}, f32[8,512,512]{2,1,0:T(8,128)}) fusion(f32[8]{0:T(128)S(1)} %get-tuple-element.251, bf16[512,8,64]{0,2,1:T(8,128)(2,1)S(1)} %get-tuple-element.250, bf16[2,2048,8,64]{1,3,2,0:T(8,128)(2,1)} %get-tuple-element.249, s32[]{:T(128)S(6)} %select_n.481), kind=kOutput, calls=%fused_computation.8.clone.1 | convolution fusion | flops 287309824 | bytes 17825828 | tf_op jit(solution)/shard_map/while/body/eval_jaxpr/thd,khd->htk/dot_general | solution.py:31
  255.5 11.5 %fusion.119 = f32[8,512,4,128]{1,0,3,2:T(8,128)} fusion(f32[8,512,4,128]{1,3,2,0:T(8,128)} %bitcast.152), kind=kOutput, calls=%fused_computation.16.clone.1 | output fusion | flops 266338304 | bytes 16777216 | tf_op jit(solution)/shard_map/reduce-window.6
  267.0 0.8 fusion.120
  267.9 4.4 %broadcast_add_fusion.3 = f32[8,512,4,128]{1,0,3,2:T(8,128)S(1)} fusion(f32[8,512,4,128]{1,0,3,2:T(8,128)} %fusion.119, f32[8,512,4]{1,0,2:T(8,128)S(1)} %slice.317), kind=kLoop, calls=%fused_computation.19.clone.1 | loop fusion | flops 2097152 | bytes 16842752 | tf_op jit(solution)/shard_map/reduce_window_sum
  272.3 4.9 %copy.54 = f32[8,512,4,128]{1,3,2,0:T(8,128)S(1)} copy(f32[8,512,4,128]{1,0,3,2:T(8,128)S(1)} %broadcast_add_fusion.3) | data formatting | bytes 16777216 | tf_op jit(solution)/shard_map/reduce_window_sum
  277.2 3.2 copy-done.2
  280.4 11.2 %fusion.121 = f32[512,8,64]{0,2,1:T(8,128)S(1)} fusion(f32[512,8,64]{0,2,1:T(8,128)S(1)} %get-tuple-element.234, f32[8,512,512]{1,2,0:T(8,128)} %bitcast.151, f32[8,512,512]{2,1,0:T(8,128)} %get-tuple-element.220, f32[8,512]{1,0:T(8,128)S(1)} %get-tuple-element.235, f32[8,512]{1,0:T(8,128)S(1)} %bitcast.164, f32[8]{0:T(128)S(1)} %get-tuple-element.251, ...), kind=kOutput, calls=%fused_computation.23.clone.1 | convolution fusion | flops 298319872 | bytes 19431464 | tf_op jit(solution)/shard_map/while/body/eval_jaxpr/htk,khd->thd/dot_general | solution.py:52
  291.7 10.4 %fusion.118 = (f32[8,512,512]{1,2,0:T(8,128)}, f32[8,512,512]{2,1,0:T(8,128)}) fusion(f32[8]{0:T(128)S(1)} %get-tuple-element.251, bf16[512,8,64]{0,2,1:T(8,128)(2,1)S(1)} %get-tuple-element.250, bf16[2,2048,8,64]{1,3,2,0:T(8,128)(2,1)} %get-tuple-element.249, s32[]{:T(128)S(6)} %select_n.481), kind=kOutput, calls=%fused_computation.8.clone.1 | convolution fusion | flops 287309824 | bytes 17825828 | tf_op jit(solution)/shard_map/while/body/eval_jaxpr/thd,khd->htk/dot_general | solution.py:31
  302.1 11.5 %fusion.119 = f32[8,512,4,128]{1,0,3,2:T(8,128)} fusion(f32[8,512,4,128]{1,3,2,0:T(8,128)} %bitcast.152), kind=kOutput, calls=%fused_computation.16.clone.1 | output fusion | flops 266338304 | bytes 16777216 | tf_op jit(solution)/shard_map/reduce-window.6
  313.6 0.8 fusion.120
  314.5 4.4 %broadcast_add_fusion.3 = f32[8,512,4,128]{1,0,3,2:T(8,128)S(1)} fusion(f32[8,512,4,128]{1,0,3,2:T(8,128)} %fusion.119, f32[8,512,4]{1,0,2:T(8,128)S(1)} %slice.317), kind=kLoop, calls=%fused_computation.19.clone.1 | loop fusion | flops 2097152 | bytes 16842752 | tf_op jit(solution)/shard_map/reduce_window_sum
  318.9 4.9 %copy.54 = f32[8,512,4,128]{1,3,2,0:T(8,128)S(1)} copy(f32[8,512,4,128]{1,0,3,2:T(8,128)S(1)} %broadcast_add_fusion.3) | data formatting | bytes 16777216 | tf_op jit(solution)/shard_map/reduce_window_sum
  323.8 3.2 copy-done.2
  327.0 11.0 %fusion.121 = f32[512,8,64]{0,2,1:T(8,128)S(1)} fusion(f32[512,8,64]{0,2,1:T(8,128)S(1)} %get-tuple-element.234, f32[8,512,512]{1,2,0:T(8,128)} %bitcast.151, f32[8,512,512]{2,1,0:T(8,128)} %get-tuple-element.220, f32[8,512]{1,0:T(8,128)S(1)} %get-tuple-element.235, f32[8,512]{1,0:T(8,128)S(1)} %bitcast.164, f32[8]{0:T(128)S(1)} %get-tuple-element.251, ...), kind=kOutput, calls=%fused_computation.23.clone.1 | convolution fusion | flops 298319872 | bytes 19431464 | tf_op jit(solution)/shard_map/while/body/eval_jaxpr/htk,khd->thd/dot_general | solution.py:52
  338.1 10.4 %fusion.118 = (f32[8,512,512]{1,2,0:T(8,128)}, f32[8,512,512]{2,1,0:T(8,128)}) fusion(f32[8]{0:T(128)S(1)} %get-tuple-element.251, bf16[512,8,64]{0,2,1:T(8,128)(2,1)S(1)} %get-tuple-element.250, bf16[2,2048,8,64]{1,3,2,0:T(8,128)(2,1)} %get-tuple-element.249, s32[]{:T(128)S(6)} %select_n.481), kind=kOutput, calls=%fused_computation.8.clone.1 | convolution fusion | flops 287309824 | bytes 17825828 | tf_op jit(solution)/shard_map/while/body/eval_jaxpr/thd,khd->htk/dot_general | solution.py:31
  348.6 11.5 %fusion.119 = f32[8,512,4,128]{1,0,3,2:T(8,128)} fusion(f32[8,512,4,128]{1,3,2,0:T(8,128)} %bitcast.152), kind=kOutput, calls=%fused_computation.16.clone.1 | output fusion | flops 266338304 | bytes 16777216 | tf_op jit(solution)/shard_map/reduce-window.6
  360.1 0.8 fusion.120
  360.9 4.4 %broadcast_add_fusion.3 = f32[8,512,4,128]{1,0,3,2:T(8,128)S(1)} fusion(f32[8,512,4,128]{1,0,3,2:T(8,128)} %fusion.119, f32[8,512,4]{1,0,2:T(8,128)S(1)} %slice.317), kind=kLoop, calls=%fused_computation.19.clone.1 | loop fusion | flops 2097152 | bytes 16842752 | tf_op jit(solution)/shard_map/reduce_window_sum
  365.4 4.9 %copy.54 = f32[8,512,4,128]{1,3,2,0:T(8,128)S(1)} copy(f32[8,512,4,128]{1,0,3,2:T(8,128)S(1)} %broadcast_add_fusion.3) | data formatting | bytes 16777216 | tf_op jit(solution)/shard_map/reduce_window_sum
  370.2 3.2 copy-done.2
  373.5 11.0 %fusion.121 = f32[512,8,64]{0,2,1:T(8,128)S(1)} fusion(f32[512,8,64]{0,2,1:T(8,128)S(1)} %get-tuple-element.234, f32[8,512,512]{1,2,0:T(8,128)} %bitcast.151, f32[8,512,512]{2,1,0:T(8,128)} %get-tuple-element.220, f32[8,512]{1,0:T(8,128)S(1)} %get-tuple-element.235, f32[8,512]{1,0:T(8,128)S(1)} %bitcast.164, f32[8]{0:T(128)S(1)} %get-tuple-element.251, ...), kind=kOutput, calls=%fused_computation.23.clone.1 | convolution fusion | flops 298319872 | bytes 19431464 | tf_op jit(solution)/shard_map/while/body/eval_jaxpr/htk,khd->thd/dot_general | solution.py:52
  384.6 0.2 convert_convert_fusion
  384.8 2.5 all-reduce
  387.2 0.2 fusion.54
  387.5 4.0 fusion.81
  391.5 5.5 %add_convert_fusion = bf16[512,2048]{1,0:T(8,128)(2,1)} fusion(f32[512,2048]{1,0:T(8,128)} %fusion.81, bf16[512,512]{0,1:T(8,128)(2,1)S(1)} %fusion.54, bf16[512,2048]{1,0:T(8,128)(2,1)} %all-gather.23.cloned.1.call-done), kind=kOutput, calls=%fused_computation.57 | convolution fusion | flops 1075838976 | bytes 8912896 | tf_op jit(solution)/shard_map/dot_general | solution.py:162
  397.0 8.6 %reduce-scatter.2.cloned.1.call-done = bf16[256,2048]{1,0:T(8,128)(2,1)} async-done(((bf16[512,2048]{1,0:T(8,128)(2,1)}), bf16[256,2048]{1,0:T(8,128)(2,1)}) %reduce-scatter.2.cloned.1.call-update) | async-done | bytes 1048592 | tf_op jit(solution)/shard_map/reduce_scatter | solution.py:159
  (84 shorter events, 0.8 us)
Async XLA Ops:
  6.5 126.2 %copy-start = (bf16[2,128,128]{2,1,0:T(8,128)(2,1)S(1)}, bf16[2,128,128]{2,1,0:T(8,128)(2,1)}, u32[]{:S(2)}) copy-start(bf16[2,128,128]{2,1,0:T(8,128)(2,1)} %param.26) | copy-start | bytes 196612
  6.5 57.9 %copy-start.16 = (f32[2048]{0:T(1024)S(1)}, f32[2048]{0:T(1024)}, u32[]{:S(2)}) copy-start(f32[2048]{0:T(1024)} %param.18) | copy-start | bytes 24580
  6.5 15.7 %all-gather.9.cloned.1.call-start = ((), (), s32[]{:S(2)}) async-start(), calls=%async_computation.1 | async-start | bytes 3145728 | tf_op jit(solution)/shard_map/all_gather | solution.py:79
  7.3 53.2 %all-gather.19.cloned.1.call-start = ((), (), s32[]{:S(2)}) async-start(), calls=%async_computation.6 | async-start | bytes 2621440 | tf_op jit(solution)/shard_map/all_gather | solution.py:88
  8.0 89.5 %all-gather.15.cloned.1.call-start = ((), (), s32[]{:S(2)}) async-start(), calls=%async_computation.4 | async-start | bytes 2621440 | tf_op jit(solution)/shard_map/all_gather | solution.py:89
  8.7 117.0 %all-gather.11.cloned.1.call-start = ((), (), s32[]{:S(2)}) async-start(), calls=%async_computation.2 | async-start | bytes 1310720 | tf_op jit(solution)/shard_map/all_gather | solution.py:86
  9.3 153.3 %all-gather.17.cloned.1.call-start = ((), (), s32[]{:S(2)}) async-start(), calls=%async_computation.5 | async-start | bytes 2621440 | tf_op jit(solution)/shard_map/all_gather | solution.py:87
  9.9 59.1 %copy-start.15 = (f32[64]{0:T(128)S(1)}, f32[64]{0:T(128)}, u32[]{:S(2)}) copy-start(f32[64]{0:T(128)} %param.24) | copy-start | bytes 772
  9.9 234.9 %all-gather.21.cloned.1.call-start = ((), (), s32[]{:S(2)}) async-start(), calls=%async_computation.7 | async-start | bytes 5242880 | tf_op jit(solution)/shard_map/all_gather | solution.py:131
  24.3 73.2 %copy-start.3 = (bf16[1,512,2048]{2,1,0:T(8,128)(2,1)S(1)}, bf16[1,512,2048]{2,1,0:T(8,128)(2,1)}, u32[]{:S(2)}) copy-start(bf16[1,512,2048]{2,1,0:T(8,128)(2,1)} %all-gather.9.cloned.1.call-done) | copy-start | bytes 6291460
  68.0 1.0 copy-start.5
  69.2 62.4 %copy-start.17 = (bf16[256]{0:T(256)(128)(2,1)S(1)}, bf16[256]{0:T(256)(128)(2,1)}, u32[]{:S(2)}) copy-start(bf16[256]{0:T(256)(128)(2,1)} %param.28) | copy-start | bytes 1540
  69.2 62.9 %copy-start.13 = (bf16[512]{0:T(512)(128)(2,1)S(1)}, bf16[512]{0:T(512)(128)(2,1)}, u32[]{:S(2)}) copy-start(bf16[512]{0:T(512)(128)(2,1)} %param.29) | copy-start | bytes 3076
  69.2 63.5 %copy-start.12 = (f32[256]{0:T(256)S(1)}, f32[256]{0:T(256)}, u32[]{:S(2)}) copy-start(f32[256]{0:T(256)} %param.27) | copy-start | bytes 3076
  100.5 0.8 copy-start.7
  102.4 285.0 %all-gather.13.cloned.1.call-start = ((), (), s32[]{:S(2)}) async-start(), calls=%async_computation.3 | async-start | bytes 1310720 | tf_op jit(solution)/shard_map/all_gather | solution.py:149
  103.2 288.3 %all-gather.23.cloned.1.call-start = ((), (), s32[]{:S(2)}) async-start(), calls=%async_computation.8 | async-start | bytes 2621440 | tf_op jit(solution)/shard_map/all_gather | solution.py:150
  103.9 301.7 %reduce-scatter.2.cloned.1.call-start = ((), (), s32[]{:S(2)}) async-start(), calls=%async_computation.9 | async-start | bytes 3145728 | tf_op jit(solution)/shard_map/reduce_scatter | solution.py:159
  127.7 5.0 %collective-permute-start = (bf16[16,256]{1,0:T(8,128)(2,1)S(1)}, bf16[16,256]{1,0:T(8,128)(2,1)S(1)}, u32[]{:S(2)}, u32[]{:S(2)}) collective-permute-start(bf16[16,256]{1,0:T(8,128)(2,1)S(1)} %slice.115), channel_id=1, source_target_pairs={{0,8},{8,16},{16,24},{1,9},{9,17},{17,25},{2,10},{10,18},{18,26},{... | collective-permute-start | bytes 24584 | tf_op jit(solution)/shard_map/ppermute | solution.py:20
  134.9 34.6 %copy-start.14 = (f32[64]{0:T(128)S(1)}, f32[64]{0:T(128)}, u32[]{:S(2)}) copy-start(f32[64]{0:T(128)} %param.23) | copy-start | bytes 772
  134.9 34.9 %copy-start.6 = (f32[512,8,64]{0,2,1:T(8,128)S(1)}, f32[512,8,64]{0,2,1:T(8,128)}, u32[]{:S(2)}) copy-start(f32[512,8,64]{0,2,1:T(8,128)} %copy-done.5) | copy-start | bytes 3145732
  134.9 34.9 %copy-start.18 = (f32[8]{0:T(128)S(1)}, f32[8]{0:T(128)}, u32[]{:S(2)}) copy-start(f32[8]{0:T(128)} %param.25) | copy-start | bytes 100
  196.9 4.9 %copy-start.8 = (bf16[512,512]{0,1:T(8,128)(2,1)S(1)}, bf16[512,512]{0,1:T(8,128)(2,1)}, u32[]{:S(2)}) copy-start(bf16[512,512]{0,1:T(8,128)(2,1)} %copy-done.7) | copy-start | bytes 1572868
  244.8 139.9 %copy-start.11 = (f32[512]{0:T(512)S(1)}, f32[512]{0:T(512)}, u32[]{:S(2)}) copy-start(f32[512]{0:T(512)} %get-tuple-element.150) | copy-start | bytes 6148
  244.8 142.4 %copy-start.9 = (f32[512]{0:T(512)S(1)}, f32[512]{0:T(512)}, u32[]{:S(2)}) copy-start(f32[512]{0:T(512)} %convert_element_type.117) | copy-start | bytes 6148
  244.8 142.6 %copy-start.4 = (bf16[512,256]{0,1:T(8,128)(2,1)S(1)}, bf16[512,256]{0,1:T(8,128)(2,1)}, u32[]{:S(2)}) copy-start(bf16[512,256]{0,1:T(8,128)(2,1)} %fusion.78) | copy-start | bytes 786436
  244.8 142.6 %copy-start.10 = (f32[256]{0:T(256)S(1)}, f32[256]{0:T(256)}, u32[]{:S(2)}) copy-start(f32[256]{0:T(256)} %convert_element_type.104) | copy-start | bytes 3076
  277.2 3.2 copy-start.2
  323.8 3.2 copy-start.2
  370.2 3.2 copy-start.2
  387.5 18.2 %copy-start.1 = (bf16[2,128,128]{2,1,0:T(8,128)(2,1)S(1)}, bf16[2,128,128]{2,1,0:T(8,128)(2,1)}, u32[]{:S(2)}) copy-start(bf16[2,128,128]{2,1,0:T(8,128)(2,1)} %param.26) | copy-start | bytes 196612
Sparse Core Ops, SparseCore 0:
  8.9 13.2 all-gather.8
  24.1 36.3 all-gather.18
  62.3 35.1 all-gather.14
  99.2 26.4 all-gather.10
  127.4 35.1 all-gather.16
  164.0 80.7 all-gather.20
  246.6 24.8 all-gather.12
  273.4 35.0 all-gather.22
  397.1 8.4 reduce-scatter.1
where the time goes:
time: 418 us; the launch traced here: 413 us
  waiting for transfers between devices  172 us (41%)
  matrix products  107 us (26%)
  other arithmetic  73.3 us (18%)
  local copies, waits for them, and re-layouts  38.9 us (9%)
  between operations  14 us (3%)
    another operation x12, other arithmetic  67.2 us
    dot_general x4, matrix products, stick_block(): jnp.einsum('htk,khd->thd', weight, value_heads, preferred_element_type=jn...  42.8 us
    dot_general x4, matrix products, stick_block(): jnp.einsum('thd,khd->htk', query, key_heads, preferred_element_type=jnp.f...  41.5 us
    all_gather x1, waiting for transfers between devices, shards(): lax.all_gather(w_key, 'fs', axis=0, tiled=True)  36.1 us
    all_gather x1, waiting for transfers between devices, shards(): everything = lax.all_gather(key_value, 'sp', axis=1, tiled=True)  33.6 us
    all_gather x1, waiting for transfers between devices, shards(): lax.all_gather(w_value, 'fs', axis=0, tiled=True)  28.3 us
    all_gather x1, waiting for transfers between devices, shards(): lax.all_gather(w_query, 'fs', axis=0, tiled=True)  26.9 us
    all_gather x1, waiting for transfers between devices, shards(): lax.all_gather(w_pool_in, 'fs', axis=0, tiled=True)  21.5 us
  transfers between devices with their start and end apart: 10, of which 7 were waited for; matrix products, arithmetic and copies ran while one was open for 49% of the time, Pallas kernels for 0%

commit v1 on v0

--- a/solution.py
+++ b/solution.py
@@ -3,6 +3,8 @@
 import jax
 import jax.numpy as jnp
 from jax import lax
+from jax.experimental import pallas as pl
+from jax.experimental.pallas import tpu as pltpu
 from jax.sharding import PartitionSpec as P
 
 HEADS = 16
@@ -168,6 +170,409 @@
     return mixed[None]
 
 
+F32 = jnp.float32
+BF = jnp.bfloat16
+HALO = 16
+
+
+def fused_kernel(
+    tok, ng, wp, wq, wk, wv, qg, kg, off, mix, psc, pgain, again, wop, woa,
+    out,
+    tokf, normed, gk, gv, gq, gp, gop, goa,
+    qloc, kloc, vloc, qb, kb, vb, oloc, ob,
+    pin, halo, pooled, sqs, act, snd, rcv,
+    lsem, wss, wrs, ass, ars, oss, ors, fss, frs, mss, mrs,
+):
+    sp_n = lax.axis_size("sp")
+    fs_n = lax.axis_size("fs")
+    me_sp, me_fs, me_tp = lax.axis_index("sp"), lax.axis_index("fs"), lax.axis_index("tp")
+    near_x = me_fs + 1 - 2 * (me_fs % 2)
+    near_y = (me_fs + 2) % fs_n
+    other = 1 - me_tp
+    rows, half_d = tok.shape
+    qblk = qb.shape[1]
+    lane = lax.broadcasted_iota(jnp.int32, (1, 2 * HEAD_DIM), 1)
+    first = lane < HEAD_DIM
+
+    items = ((wk, gk), (wv, gv), (wq, gq), (wp, gp), (wop, gop), (woa, goa))
+    local = [pltpu.make_async_copy(src, g.at[me_fs], lsem.at[i]) for i, (src, g) in enumerate(items)]
+    tok_local = pltpu.make_async_copy(tok, tokf.at[me_tp], lsem.at[6])
+    tok_local.start()
+    for copy in local:
+        copy.start()
+
+    barrier = pltpu.get_barrier_semaphore()
+    greet = [{"fs": near_x}, {"fs": near_y}, {"tp": other}]
+    greet += [{"sp": (me_sp + d) % sp_n} for d in range(1, sp_n)]
+    for target in greet:
+        pl.semaphore_signal(barrier, inc=1, device_id=target, device_id_type=pl.DeviceIdType.MESH)
+    pl.semaphore_wait(barrier, len(greet))
+
+    def remote(src, dst, send, recv, target):
+        return pltpu.make_async_remote_copy(
+            src_ref=src, dst_ref=dst, send_sem=send, recv_sem=recv,
+            device_id=target, device_id_type=pl.DeviceIdType.MESH,
+        )
+
+    tok_copy = remote(tokf.at[me_tp], tokf.at[me_tp], mss.at[0], mrs.at[0], {"tp": other})
+    tok_local.wait()
+    tok_copy.start()
+
+    def weight_copies(i):
+        g = items[i][1]
+        half = g.shape[1] // 2
+        lower, upper = pl.ds(0, half), pl.ds(half, half)
+        own_x = remote(g.at[me_fs], g.at[me_fs], wss.at[i, 0], wrs.at[i, 0], {"fs": near_x})
+        own_y = remote(g.at[me_fs], g.at[me_fs], wss.at[i, 1], wrs.at[i, 1], {"fs": near_y})
+        pass_y = remote(
+            g.at[near_x, lower], g.at[near_x, lower], wss.at[i, 2], wrs.at[i, 2], {"fs": near_y}
+        )
+        pass_x = remote(
+            g.at[near_y, upper], g.at[near_y, upper], wss.at[i, 3], wrs.at[i, 3], {"fs": near_x}
+        )
+        return own_x, own_y, pass_y, pass_x
+
+    copies = [weight_copies(i) for i in range(len(items))]
+
+    def send_own(i):
+        local[i].wait()
+        copies[i][0].start()
+        copies[i][1].start()
+
+    def pass_on(i):
+        copies[i][0].wait_recv()
+        copies[i][2].start()
+        copies[i][1].wait_recv()
+        copies[i][3].start()
+
+    def arrived(i):
+        copies[i][2].wait_recv()
+        copies[i][3].wait_recv()
+
+    send_own(0)
+    send_own(1)
+
+    tok_copy.wait_recv()
+    chunk = 128
+    width = normed.shape[2]
+
+    def norm_rows(c, carry):
+        at = pl.ds(pl.multiple_of(c * chunk, chunk), chunk)
+        parts = [tokf[t, at, :].astype(F32) for t in range(2)]
+        total = sum(jnp.sum(p * p, axis=-1, keepdims=True) for p in parts)
+        factor = lax.rsqrt(total / (2 * half_d) + EPS)
+        for f in range(fs_n):
+            t, begin = divmod(f * width, half_d)
+            piece = parts[t][:, begin : begin + width]
+            gain = ng[:, f * width : (f + 1) * width]
+            normed[f, at, :] = (piece * factor * gain).astype(BF)
+        return carry
+
+    lax.fori_loop(0, rows // chunk, norm_rows, 0)
+
+    def project(g, finish):
+        def body(r, carry):
+            at = pl.ds(pl.multiple_of(r * qblk, qblk), qblk)
+            acc = jnp.dot(normed[0, at, :], g[0], preferred_element_type=F32)
+            for f in range(1, fs_n):
+                acc = acc + jnp.dot(normed[f, at, :], g[f], preferred_element_type=F32)
+            finish(r, acc)
+            return carry
+
+        lax.fori_loop(0, rows // qblk, body, 0)
+
+    blocks = rows // qblk
+
+    def to_heads(dest, gain, scale):
+        def finish(r, acc):
+            for j in range(sp_n):
+                x = acc[:, j * 2 * HEAD_DIM : (j + 1) * 2 * HEAD_DIM]
+                if gain is not None:
+                    sq = x * x
+                    low = jnp.sum(jnp.where(first, sq, 0.0), axis=-1, keepdims=True)
+                    high = jnp.sum(jnp.where(first, 0.0, sq), axis=-1, keepdims=True)
+                    mean = jnp.where(first, low, high) / HEAD_DIM
+                    x = x * lax.rsqrt(mean + EPS) * gain[...]
+                y = x.astype(BF)
+                if scale is not None:
+                    y = y * jnp.asarray(scale, BF)
+                dest[j * blocks + r] = y
+
+        return finish
+
+    def exchange(i, src, dst):
+        mine = pl.ds(me_sp * blocks, blocks)
+        keep = pltpu.make_async_copy(src.at[mine], dst.at[mine], lsem.at[7 + i])
+        sends = []
+        for d in range(1, sp_n):
+            peer = (me_sp + d) % sp_n
+            sends.append(
+                remote(
+                    src.at[pl.ds(peer * blocks, blocks)], dst.at[mine],
+                    ass.at[i, d - 1], ars.at[i, d - 1], {"sp": peer},
+                )
+            )
+        return keep, sends
+
+    swaps = [exchange(0, kloc, kb), exchange(1, vloc, vb), exchange(2, qloc, qb)]
+
+    def start_swap(i):
+        swaps[i][0].start()
+        for copy in swaps[i][1]:
+            copy.start()
+
+    pass_on(0)
+    pass_on(1)
+    send_own(2)
+    arrived(0)
+    project(gk, to_heads(kloc, kg, None))
+    start_swap(0)
+    arrived(1)
+    project(gv, to_heads(vloc, None, None))
+    start_swap(1)
+    pass_on(2)
+    send_own(3)
+    arrived(2)
+    project(gq, to_heads(qloc, qg, 1.0 / math.sqrt(HEAD_DIM)))
+    start_swap(2)
+    pass_on(3)
+    send_own(4)
+    send_own(5)
+    arrived(3)
+
+    def keep_pool(r, acc):
+        pin[pl.ds(pl.multiple_of(r * qblk, qblk), qblk), :] = acc.astype(BF)
+
+    project(gp, keep_pool)
+    halo_copy = remote(
+        pin.at[pl.ds(rows - HALO, HALO)], halo, mss.at[1], mrs.at[1], {"sp": (me_sp + 1) % sp_n}
+    )
+    halo_copy.start()
+    halo_copy.wait_recv()
+    before = jnp.where(me_sp > 0, halo[...].astype(F32), 0.0)
+    position = me_sp * rows + lax.broadcasted_iota(jnp.int32, (rows, 1), 0)
+    pool_sq = jnp.zeros((rows, 1), F32)
+    group_ch = mix.shape[1]
+    for grp in range(mix.shape[0]):
+        cols = slice(grp * group_ch, (grp + 1) * group_ch)
+        ext = jnp.concatenate([before[:, cols], pin[:, cols].astype(F32)], axis=0)
+        group_id = me_tp * mix.shape[0] + grp
+        summed = ext
+        picked = jnp.zeros_like(ext)
+        for level in range(POOL_GROUPS):
+            summed = summed + pltpu.roll(summed, 1 << level, 0)
+            picked = jnp.where(group_id == level, summed, picked)
+        window = jnp.where(group_id == 0, 2, jnp.where(group_id == 1, 4, jnp.where(group_id == 2, 8, 16)))
+        counted = jnp.minimum(position + 1, window).astype(F32)
+        centered = (picked[HALO:] / counted - ext[HALO:]).astype(BF)
+        mixed = jnp.dot(centered, mix[grp], preferred_element_type=F32) * psc[:, cols]
+        kept = mixed.astype(BF)
+        pooled[:, cols] = kept
+        kept_f = kept.astype(F32)
+        pool_sq = pool_sq + jnp.sum(kept_f * kept_f, axis=-1, keepdims=True)
+    sqs[0] = jnp.where(first, pool_sq, 0.0)
+
+    for keep, sends in swaps:
+        keep.wait()
+        for copy in sends:
+            copy.wait_recv()
+
+    key_id = lax.broadcasted_iota(jnp.int32, (qblk, qblk), 0)
+    col_id = lax.broadcasted_iota(jnp.int32, (qblk, qblk), 1)
+    after = (key_id > col_id).astype(F32).astype(BF)
+    offsets = [off[2 * me_sp + h] for h in range(2)]
+
+    def attend(qi):
+        query = qb[qi]
+        zero = jnp.zeros_like(query)
+        queries = (jnp.where(first, query, zero), jnp.where(first, zero, query))
+
+        def block(kj, state, masked):
+            key, val = kb[kj], vb[kj]
+            result = []
+            for h in range(2):
+                acc, carry = state[2 * h], state[2 * h + 1]
+                z = lax.dot_general(
+                    queries[h], key, (((1,), (1,)), ((), ())), preferred_element_type=F32
+                ) + offsets[h]
+                soft = jnp.log(1.0 + jnp.exp(z))
+                log_own = z - soft
+                if masked:
+                    soft = jnp.where(col_id < key_id, soft, 0.0)
+                later = jnp.dot(soft.astype(BF), after, preferred_element_type=F32)
+                weight = jnp.exp(log_own - later - carry)
+                if masked:
+                    weight = jnp.where(col_id < key_id, weight, 0.0)
+                acc = acc + jnp.dot(weight.astype(BF), val, preferred_element_type=F32)
+                carry = carry + later[:, :1] + soft[:, :1]
+                result += [acc, carry]
+            return tuple(result)
+
+        start = (jnp.zeros((qblk, 2 * HEAD_DIM), F32), jnp.zeros((qblk, 1), F32)) * 2
+        state = block(qi, start, True)
+        state = lax.fori_loop(0, qi, lambda n, s: block(qi - 1 - n, s, False), state)
+        oloc[qi] = jnp.where(first, state[0], state[2]).astype(BF)
+
+    def attend_rows(d):
+        place = (me_sp + d) % sp_n
+
+        def one(r, carry):
+            attend(place * blocks + r)
+            return carry
+
+        lax.fori_loop(0, blocks, one, 0)
+
+    def give_back(d):
+        place = (me_sp + d) % sp_n
+        return remote(
+            oloc.at[pl.ds(place * blocks, blocks)], ob.at[pl.ds(me_sp * blocks, blocks)],
+            oss.at[d - 1], ors.at[d - 1], {"sp": place},
+        )
+
+    attend_rows(1)
+    give_back(1).start()
+    pass_on(4)
+    pass_on(5)
+
+    def middle(d, carry):
+        attend_rows(d)
+        give_back(d).start()
+        return carry
+
+    lax.fori_loop(2, sp_n, middle, 0)
+    attend_rows(sp_n)
+    mine = pl.ds(me_sp * blocks, blocks)
+    keep_out = pltpu.make_async_copy(oloc.at[mine], ob.at[mine], lsem.at[10])
+    keep_out.start()
+    keep_out.wait()
+    for d in range(1, sp_n):
+        give_back(d).wait_recv()
+
+    attn_sq = jnp.zeros((rows, 1), F32)
+    attended = [ob[j * blocks : (j + 1) * blocks].reshape(rows, 2 * HEAD_DIM).astype(F32) for j in range(sp_n)]
+    for piece in attended:
+        attn_sq = attn_sq + jnp.sum(piece * piece, axis=-1, keepdims=True)
+    sqs[0] = jnp.where(first, sqs[0], attn_sq)
+    sq_copy = remote(sqs.at[0], sqs.at[1], mss.at[2], mrs.at[2], {"tp": other})
+    sq_copy.start()
+    arrived(4)
+    arrived(5)
+    sq_copy.wait_recv()
+    totals = sqs[0] + sqs[1]
+    pool_ch = pooled.shape[1]
+    attn_ch = goa.shape[1]
+    pool_factor = lax.rsqrt(totals[:, :1] / (2 * pool_ch) + EPS)
+    attn_factor = lax.rsqrt(totals[:, HEAD_DIM : HEAD_DIM + 1] / (2 * attn_ch) + EPS)
+    act[:, :pool_ch] = (pooled[...].astype(F32) * pool_factor * pgain[...]).astype(BF)
+    for j in range(sp_n):
+        cols = slice(j * 2 * HEAD_DIM, (j + 1) * 2 * HEAD_DIM)
+        spot = slice(pool_ch + j * 2 * HEAD_DIM, pool_ch + (j + 1) * 2 * HEAD_DIM)
+        piece = ob[j * blocks : (j + 1) * blocks].reshape(rows, 2 * HEAD_DIM).astype(F32)
+        act[:, spot] = (piece * attn_factor * again[:, cols]).astype(BF)
+
+    share = rows // 2
+
+    def partial_sum(which, f):
+        at = pl.ds(pl.multiple_of(which * share, share), share)
+        return jnp.dot(act[at, :pool_ch], gop[f], preferred_element_type=F32) + jnp.dot(
+            act[at, pool_ch:], goa[f], preferred_element_type=F32
+        )
+
+    def hand_over(f):
+        return remote(snd.at[f], rcv.at[f], fss.at[f], frs.at[f], {"tp": other})
+
+    def theirs(f, carry):
+        snd[f] = partial_sum(other, f).astype(BF)
+        hand_over(f).start()
+        return carry
+
+    lax.fori_loop(0, fs_n, theirs, 0)
+    out_w = gop.shape[2]
+
+    def ours(f, carry):
+        total = partial_sum(me_tp, f)
+        hand_over(f).wait_recv()
+        total = total + rcv[f].astype(F32)
+        out[:, pl.ds(pl.multiple_of(f * out_w, out_w), out_w)] = total.astype(BF)
+        return carry
+
+    lax.fori_loop(0, fs_n, ours, 0)
+
+    tok_copy.wait_send()
+    halo_copy.wait_send()
+    sq_copy.wait_send()
+    for group in copies:
+        for copy in group:
+            copy.wait_send()
+    for _, sends in swaps:
+        for copy in sends:
+            copy.wait_send()
+    for d in range(1, sp_n):
+        give_back(d).wait_send()
+    for f in range(fs_n):
+        hand_over(f).wait_send()
+
+
+def fused_shards(
+    tokens, norm_gain, w_pool_in, w_query, w_key, w_value, query_gain, key_gain,
+    stick_offset, pool_mix, pool_scale, pool_gain, attn_gain, w_out_pool, w_out_attn,
+):
+    sp_n, fs_n = lax.axis_size("sp"), lax.axis_size("fs")
+    _, rows, half_d = tokens.shape
+    depth, attn_ch = w_query.shape
+    pool_ch = w_pool_in.shape[1]
+    out_w = w_out_pool.shape[1]
+    qblk = rows // 2
+    pair = 2 * HEAD_DIM
+    nblk = sp_n * (rows // qblk)
+    vmem = pl.BlockSpec(memory_space=pltpu.VMEM)
+    hbm = pl.BlockSpec(memory_space=pl.ANY)
+    smem = pl.BlockSpec(memory_space=pltpu.SMEM)
+    dma = pltpu.SemaphoreType.DMA
+    heads = pltpu.VMEM((nblk, qblk, pair), BF)
+    result = pl.pallas_call(
+        fused_kernel,
+        out_shape=jax.ShapeDtypeStruct((rows // 2, fs_n * out_w), BF),
+        in_specs=[hbm, vmem, hbm, hbm, hbm, hbm, vmem, vmem, smem, vmem, vmem, vmem, vmem, hbm, hbm],
+        out_specs=vmem,
+        scratch_shapes=[
+            pltpu.VMEM((2, rows, half_d), BF),
+            pltpu.VMEM((fs_n, rows, depth), BF),
+            pltpu.VMEM((fs_n, depth, attn_ch), BF),
+            pltpu.VMEM((fs_n, depth, attn_ch), BF),
+            pltpu.VMEM((fs_n, depth, attn_ch), BF),
+            pltpu.VMEM((fs_n, depth, pool_ch), BF),
+            pltpu.VMEM((fs_n, pool_ch, out_w), BF),
+            pltpu.VMEM((fs_n, attn_ch, out_w), BF),
+            heads, heads, heads, heads, heads, heads, heads, heads,
+            pltpu.VMEM((rows, pool_ch), BF),
+            pltpu.VMEM((HALO, pool_ch), BF),
+            pltpu.VMEM((rows, pool_ch), BF),
+            pltpu.VMEM((2, rows, pair), F32),
+            pltpu.VMEM((rows, pool_ch + attn_ch), BF),
+            pltpu.VMEM((fs_n, rows // 2, out_w), BF),
+            pltpu.VMEM((fs_n, rows // 2, out_w), BF),
+            dma((11,)), dma((6, 4)), dma((6, 4)), dma((3, sp_n - 1)), dma((3, sp_n - 1)),
+            dma((sp_n - 1,)), dma((sp_n - 1,)), dma((fs_n,)), dma((fs_n,)), dma((3,)), dma((3,)),
+        ],
+        compiler_params=pltpu.CompilerParams(
+            collective_id=0, has_side_effects=True, vmem_limit_bytes=60 * 1024 * 1024
+        ),
+        name="mixer",
+    )(
+        tokens[0], norm_gain[None], w_pool_in, w_query, w_key, w_value,
+        jnp.tile(query_gain, 2)[None], jnp.tile(key_gain, 2)[None], stick_offset, pool_mix,
+        pool_scale[None], pool_gain.astype(F32)[None], attn_gain.astype(F32)[None],
+        w_out_pool, w_out_attn,
+    )
+    return result[None]
+
+
+def suits_fused(mesh):
+    shape = mesh.shape
+    return shape["tp"] == 2 and shape["fs"] == 4 and HEADS // shape["tp"] == 2 * shape["sp"]
+
+
 def solution(mesh):
     in_specs = (
         P("fs", "sp", "tp"),
@@ -187,4 +592,5 @@
         P("tp", "fs"),
     )
     out_specs = P("fs", ("sp", "tp"), None)
-    return jax.shard_map(shards, mesh=mesh, in_specs=in_specs, out_specs=out_specs, check_vma=False)
+    body = fused_shards if suits_fused(mesh) else shards
+    return jax.shard_map(body, mesh=mesh, in_specs=in_specs, out_specs=out_specs, check_vma=False)

time: 418 us -> 122 us (0.29); the launches traced: 413 us -> 122 us
  waiting for transfers between devices: 172 us -> 0 us
  Pallas kernels: 0 us -> 115 us
  matrix products: 107 us -> 0 us
  other arithmetic: 73.3 us -> 1.16 us
  local copies, waits for them, and re-layouts: 38.9 us -> 4.96 us
  between operations: 14 us -> 0.02 us
    all_gather x8 -> x0, waiting for transfers between devices: 159 us -> none  [the longest x1 36.1 us: shards(): lax.all_gather(w_key, 'fs', axis=0, tiled=True)]
    pallas_call x0 -> x1, Pallas kernels: none -> 115 us  [fused_shards(): pl.pallas_call(fused_kernel, out_shape=jax.ShapeDtypeStruct((rows // 2, f...]
    dot_general x15 -> x0, matrix products: 107 us -> none  [the longest x4 42.8 us: stick_block(): jnp.einsum('htk,khd->thd', weight, value_heads, preferred_element_type=jn...]
    another operation x14 -> x0, other arithmetic: 68.5 us -> none
    another operation x8 -> x4, local copies, waits for them, and re-layouts: 19.4 us -> 1.32 us  [the longest x2 0.66 us: fused_shards(): jnp.tile(query_gain, 2)[None]]
    while x9 -> x0, local copies, waits for them, and re-layouts: 9.64 us -> none
    reduce_scatter x1 -> x0, waiting for transfers between devices: 8.63 us -> none  [shards(): lax.psum_scatter((jnp.dot(pool_normed, w_pool_cols, preferred_element_typ...]
    dot_general x2 -> x0, local copies, waits for them, and re-layouts: 7.92 us -> none  [shards(): jnp.dot(normed, piece, preferred_element_type=jnp.float32)]
  transfers between devices with their start and end apart: 10 -> 0, of which waited for: 7 -> 0; matrix products, arithmetic and copies ran while one was open for 49% -> 0% of each run, Pallas kernels for 0% -> 0%
where the time goes in v1:
time: 122 us
  Pallas kernels  115 us (94%)
  local copies, waits for them, and re-layouts  4.96 us (4%)
    pallas_call x1, Pallas kernels, fused_shards(): pl.pallas_call(fused_kernel, out_shape=jax.ShapeDtypeStruct((rows // 2, f...  115 us
    unnamed x9, local copies, waits for them, and re-layouts  3.65 us

profile of v1, /device:TPU:0, one launch (start us, length us, event | category | flops | bytes accessed | tf_op | source)
XLA Modules:
  0.0 121.6 jit_solution(16740140304015341901)
XLA Ops:
  0.0 0.0 copy-start.1
  0.0 0.7 copy-done.1
  0.7 0.0 copy-start.2
  0.7 0.7 broadcast_in_dim_tile.6.qg
  1.3 0.0 copy-done.2
  1.3 0.0 copy-start.3
  1.3 0.7 broadcast_in_dim_tile.7.kg
  2.0 0.0 copy-done.3
  2.0 0.6 broadcast_in_dim.26
  2.6 0.0 copy-start
  2.6 0.7 copy-done
  3.2 0.6 broadcast_in_dim.27
  3.8 115.4 %mixer.1 = bf16[256,2048]{1,0:T(8,128)(2,1)} custom-call(bf16[512,1024]{1,0:T(8,128)(2,1)} %bitcast.7, f32[1,2048]{1,0:T(1,128)} %bitcast.8, bf16[512,256]{1,0:T(8,128)(2,1)} %wp.1, bf16[512,512]{1,0:T(8,128)(2,1)} %wq.1, bf16[512,512]{1,0:T(8,128)(2,1)} %wk.1, bf16[512,512]{1,0:T(8,128)(2,1)} %wv.1, f32[1,128]{1,0:T(1,128)} %broadcast_in_dim_tile.6.qg, ...), custom_call_target="tpu_custom_call" | custom-call | tf_op jit(solution)/shard_map/mixer/pallas_call | solution.py:533
  119.2 2.3 %copy.17 = bf16[1,256,2048]{2,1,0:T(8,128)(2,1)} copy(bf16[1,256,2048]{2,1,0:T(8,128)(2,1)} %bitcast.6) | data formatting | bytes 2097152
  (2 shorter events, 0.0 us)
Async XLA Ops:
  0.0 0.7 copy-start.1
  0.7 0.7 copy-start.2
  1.3 0.7 copy-start.3
  2.6 0.7 copy-start

commit v2 on v1

--- a/solution.py
+++ b/solution.py
@@ -194,6 +194,14 @@
     lane = lax.broadcasted_iota(jnp.int32, (1, 2 * HEAD_DIM), 1)
     first = lane < HEAD_DIM
 
+    def row(ref, begin, size):
+        return ref[begin : begin + size].astype(F32)[None, :]
+
+    def twice(ref):
+        single = row(ref, 0, HEAD_DIM)
+        return jnp.concatenate([single, single], axis=1)
+
+
     items = ((wk, gk), (wv, gv), (wq, gq), (wp, gp), (wop, gop), (woa, goa))
     local = [pltpu.make_async_copy(src, g.at[me_fs], lsem.at[i]) for i, (src, g) in enumerate(items)]
     tok_local = pltpu.make_async_copy(tok, tokf.at[me_tp], lsem.at[6])
@@ -232,7 +240,47 @@
         )
         return own_x, own_y, pass_y, pass_x
 
-    copies = [weight_copies(i) for i in range(len(items))]
+    plane = me_sp % 2
+    full_peer = me_fs + (1 - plane) * (near_x - me_fs) + plane * (near_y - me_fs)
+    half_peer = me_fs + (1 - plane) * (near_y - me_fs) + plane * (near_x - me_fs)
+    diagonal = fs_n - 1 - me_fs
+    twin = me_sp + 1 - 2 * plane
+
+    def traded_copies(i):
+        g = items[i][1]
+        half = g.shape[1] // 2
+        here = pl.ds(pl.multiple_of(plane * half, half), half)
+        there = pl.ds(pl.multiple_of((1 - plane) * half, half), half)
+        plan = (
+            (me_fs, here, {"fs": full_peer}),
+            (me_fs, there, {"fs": full_peer}),
+            (me_fs, here, {"fs": half_peer}),
+            (full_peer, here, {"fs": half_peer}),
+            (full_peer, here, {"sp": twin}),
+            (diagonal, here, {"sp": twin}),
+        )
+        return [
+            remote(g.at[b, r], g.at[b, r], wss.at[i, n], wrs.at[i, n], target)
+            for n, (b, r, target) in enumerate(plan)
+        ]
+
+    traded = (0, 1, 5)
+    copies = [
+        traded_copies(i) if i in traded else weight_copies(i) for i in range(len(items))
+    ]
+
+    def trade_relay(i):
+        copies[i][0].wait_recv()
+        copies[i][3].start()
+        copies[i][4].start()
+
+    def trade_last(i):
+        copies[i][3].wait_recv()
+        copies[i][5].start()
+
+    def trade_done(i):
+        for n in (1, 2, 4, 5):
+            copies[i][n].wait_recv()
 
     def send_own(i):
         local[i].wait()
@@ -249,8 +297,12 @@
         copies[i][2].wait_recv()
         copies[i][3].wait_recv()
 
-    send_own(0)
-    send_own(1)
+    local[0].wait()
+    for n in (0, 2, 1):
+        copies[0][n].start()
+    local[1].wait()
+    for n in (0, 1):
+        copies[1][n].start()
 
     tok_copy.wait_recv()
     chunk = 128
@@ -264,7 +316,7 @@
         for f in range(fs_n):
             t, begin = divmod(f * width, half_d)
             piece = parts[t][:, begin : begin + width]
-            gain = ng[:, f * width : (f + 1) * width]
+            gain = row(ng, f * width, width)
             normed[f, at, :] = (piece * factor * gain).astype(BF)
         return carry
 
@@ -292,7 +344,7 @@
                     low = jnp.sum(jnp.where(first, sq, 0.0), axis=-1, keepdims=True)
                     high = jnp.sum(jnp.where(first, 0.0, sq), axis=-1, keepdims=True)
                     mean = jnp.where(first, low, high) / HEAD_DIM
-                    x = x * lax.rsqrt(mean + EPS) * gain[...]
+                    x = x * lax.rsqrt(mean + EPS) * gain
                 y = x.astype(BF)
                 if scale is not None:
                     y = y * jnp.asarray(scale, BF)
@@ -321,23 +373,28 @@
         for copy in swaps[i][1]:
             copy.start()
 
-    pass_on(0)
-    pass_on(1)
+    trade_relay(0)
+    copies[1][2].start()
+    trade_last(0)
+    trade_relay(1)
     send_own(2)
-    arrived(0)
-    project(gk, to_heads(kloc, kg, None))
+    trade_done(0)
+    project(gk, to_heads(kloc, twice(kg), None))
     start_swap(0)
-    arrived(1)
+    trade_last(1)
+    trade_done(1)
     project(gv, to_heads(vloc, None, None))
     start_swap(1)
     pass_on(2)
     send_own(3)
     arrived(2)
-    project(gq, to_heads(qloc, qg, 1.0 / math.sqrt(HEAD_DIM)))
+    project(gq, to_heads(qloc, twice(qg), 1.0 / math.sqrt(HEAD_DIM)))
     start_swap(2)
     pass_on(3)
     send_own(4)
-    send_own(5)
+    local[5].wait()
+    for n in (0, 2, 1):
+        copies[5][n].start()
     arrived(3)
 
     def keep_pool(r, acc):
@@ -365,7 +422,7 @@
         window = jnp.where(group_id == 0, 2, jnp.where(group_id == 1, 4, jnp.where(group_id == 2, 8, 16)))
         counted = jnp.minimum(position + 1, window).astype(F32)
         centered = (picked[HALO:] / counted - ext[HALO:]).astype(BF)
-        mixed = jnp.dot(centered, mix[grp], preferred_element_type=F32) * psc[:, cols]
+        mixed = jnp.dot(centered, mix[grp], preferred_element_type=F32) * row(psc, grp * group_ch, group_ch)
         kept = mixed.astype(BF)
         pooled[:, cols] = kept
         kept_f = kept.astype(F32)
@@ -429,17 +486,14 @@
             oss.at[d - 1], ors.at[d - 1], {"sp": place},
         )
 
-    attend_rows(1)
-    give_back(1).start()
     pass_on(4)
-    pass_on(5)
-
-    def middle(d, carry):
+    for d in range(1, sp_n):
         attend_rows(d)
         give_back(d).start()
-        return carry
-
-    lax.fori_loop(2, sp_n, middle, 0)
+        if d == 1:
+            trade_relay(5)
+        if d == 2:
+            trade_last(5)
     attend_rows(sp_n)
     mine = pl.ds(me_sp * blocks, blocks)
     keep_out = pltpu.make_async_copy(oloc.at[mine], ob.at[mine], lsem.at[10])
@@ -456,19 +510,18 @@
     sq_copy = remote(sqs.at[0], sqs.at[1], mss.at[2], mrs.at[2], {"tp": other})
     sq_copy.start()
     arrived(4)
-    arrived(5)
+    trade_done(5)
     sq_copy.wait_recv()
     totals = sqs[0] + sqs[1]
     pool_ch = pooled.shape[1]
     attn_ch = goa.shape[1]
     pool_factor = lax.rsqrt(totals[:, :1] / (2 * pool_ch) + EPS)
     attn_factor = lax.rsqrt(totals[:, HEAD_DIM : HEAD_DIM + 1] / (2 * attn_ch) + EPS)
-    act[:, :pool_ch] = (pooled[...].astype(F32) * pool_factor * pgain[...]).astype(BF)
+    act[:, :pool_ch] = (pooled[...].astype(F32) * pool_factor * row(pgain, 0, pool_ch)).astype(BF)
     for j in range(sp_n):
-        cols = slice(j * 2 * HEAD_DIM, (j + 1) * 2 * HEAD_DIM)
         spot = slice(pool_ch + j * 2 * HEAD_DIM, pool_ch + (j + 1) * 2 * HEAD_DIM)
         piece = ob[j * blocks : (j + 1) * blocks].reshape(rows, 2 * HEAD_DIM).astype(F32)
-        act[:, spot] = (piece * attn_factor * again[:, cols]).astype(BF)
+        act[:, spot] = (piece * attn_factor * row(again, j * 2 * HEAD_DIM, 2 * HEAD_DIM)).astype(BF)
 
     share = rows // 2
 
@@ -552,7 +605,7 @@
             pltpu.VMEM((rows, pool_ch + attn_ch), BF),
             pltpu.VMEM((fs_n, rows // 2, out_w), BF),
             pltpu.VMEM((fs_n, rows // 2, out_w), BF),
-            dma((11,)), dma((6, 4)), dma((6, 4)), dma((3, sp_n - 1)), dma((3, sp_n - 1)),
+            dma((11,)), dma((6, 6)), dma((6, 6)), dma((3, sp_n - 1)), dma((3, sp_n - 1)),
             dma((sp_n - 1,)), dma((sp_n - 1,)), dma((fs_n,)), dma((fs_n,)), dma((3,)), dma((3,)),
         ],
         compiler_params=pltpu.CompilerParams(
@@ -560,9 +613,8 @@
         ),
         name="mixer",
     )(
-        tokens[0], norm_gain[None], w_pool_in, w_query, w_key, w_value,
-        jnp.tile(query_gain, 2)[None], jnp.tile(key_gain, 2)[None], stick_offset, pool_mix,
-        pool_scale[None], pool_gain.astype(F32)[None], attn_gain.astype(F32)[None],
+        tokens[0], norm_gain, w_pool_in, w_query, w_key, w_value, query_gain, key_gain,
+        stick_offset, pool_mix, pool_scale, pool_gain, attn_gain,
         w_out_pool, w_out_attn,
     )
     return result[None]

time: 122 us -> 111 us (0.910); the launches traced: 122 us -> 109 us
  Pallas kernels: 115 us -> 107 us
  local copies, waits for them, and re-layouts: 4.96 us -> 2.3 us
    pallas_call x1, Pallas kernels: 115 us -> 107 us  [fused_shards(): pl.pallas_call(fused_kernel, out_shape=jax.ShapeDtypeStruct((rows // 2, f...]
    unnamed x9 -> x1, local copies, waits for them, and re-layouts: 3.65 us -> 2.3 us
    another operation x4 -> x0, local copies, waits for them, and re-layouts: 1.32 us -> none  [the longest x2 0.66 us: fused_shards(): jnp.tile(query_gain, 2)[None]]
where the time goes in v2:
time: 111 us; the launch traced here: 109 us
  Pallas kernels  107 us (96%)
  local copies, waits for them, and re-layouts  2.3 us (2%)
    pallas_call x1, Pallas kernels, fused_shards(): pl.pallas_call(fused_kernel, out_shape=jax.ShapeDtypeStruct((rows // 2, f...  107 us
    unnamed x1, local copies, waits for them, and re-layouts  2.3 us

profile of v2, /device:TPU:0, one launch (start us, length us, event | category | flops | bytes accessed | tf_op | source)
XLA Modules:
  0.0 109.2 jit_solution(6540735250391979119)
XLA Ops:
  0.0 106.9 %mixer.1 = bf16[256,2048]{1,0:T(8,128)(2,1)} custom-call(bf16[512,1024]{1,0:T(8,128)(2,1)} %bitcast.3, f32[2048]{0:T(1024)} %ng.1, bf16[512,256]{1,0:T(8,128)(2,1)} %wp.1, bf16[512,512]{1,0:T(8,128)(2,1)} %wq.1, bf16[512,512]{1,0:T(8,128)(2,1)} %wk.1, bf16[512,512]{1,0:T(8,128)(2,1)} %wv.1, f32[64]{0:T(128)} %qg.1, f32[64]{0:T(128)} %kg.1, f32[8]{0:T(128)} %off.1, ...), custom_call_target="tpu_custom_call" | custom-call | tf_op jit(solution)/shard_map/mixer/pallas_call | solution.py:586
  106.9 2.3 %copy.17 = bf16[1,256,2048]{2,1,0:T(8,128)(2,1)} copy(bf16[1,256,2048]{2,1,0:T(8,128)(2,1)} %bitcast.2) | data formatting | bytes 2097152
